TPU v7x, 32 devices: a whole 2x2x4 slice. The times are simulated.
32 devices in a mesh: grp: 2 (over y), fs: 4 (over z), tp: 4 (over x, core).
Axes of the slice: x: 2, y: 2, z: 4, core: 2. Of those that a mesh axis runs over, the one named last changes fastest.
Arguments:
- tokens: bfloat16 [3072, 2048], P(('grp', 'fs')), parts along dimension 0, may hold values from -3 to 3
- gate_weight: bfloat16 [2048, 5120], P('fs', 'tp'), may hold values from -0.125 to 0.125
- up_weight: bfloat16 [2048, 5120], P('fs', 'tp'), may hold values from -0.125 to 0.125
- down_weight: bfloat16 [5120, 2048], P('tp', 'fs'), may hold values from -0.078125 to 0.078125
- pool_weight: bfloat16 [512, 4, 512], P('fs', None, 'tp'), may hold values from -0.375 to 0.375
- pool_bias: float32 [4, 512], replicated, may hold values from -3 to 3
- pool_scale: float32 [2048], replicated, may hold values from 0.1 to 1.9
- gain_first: float32 [2048], replicated, may hold values from 0.1 to 1.9
- gain_mix: float32 [2048], replicated, may hold values from 0.1 to 1.9
- gain_second: float32 [2048], replicated, may hold values from 0.1 to 1.9
Outputs:
- result: bfloat16 [3072, 2048], P(('grp', 'fs')), parts along dimension 0
There are 2 independent parts, one for each index of `grp`. A program takes and returns all parts, laid end to end along the dimension named above; an argument that names none is the same for every part. Nothing has to cross between parts.
All inputs are finite; a program needn't handle non-finite values.
Results may differ from a plain program's by a relative error of at most 0.018.
Values may be sent and summed in bfloat16 or wider, within the bound.
A program may use at most 64 MiB of HBM per device.

v0:
```python
import jax
import jax.numpy as jnp
from jax import lax
from jax.sharding import PartitionSpec as P

eps = 1e-06
pool_spans = (2, 4, 8, 16)
pad_width = 8


def rms_scale(values, gain_vec):
    fvalues = values.astype(jnp.float32)
    scaled = fvalues * lax.rsqrt(jnp.mean(fvalues * fvalues, axis=-1, keepdims=True) + eps)
    return (scaled * gain_vec).astype(jnp.bfloat16)


def ffn_hidden(normed, gate_full, up_full):
    gate_proj = jnp.dot(normed, gate_full, preferred_element_type=jnp.float32)
    up_proj = jnp.dot(normed, up_full, preferred_element_type=jnp.float32)
    return (jax.nn.silu(gate_proj) * up_proj).astype(jnp.bfloat16)


def pool_block(padded, offset, seq_len, pool_full, pool_bias, pool_scale):
    n_tokens = padded.shape[0] - 2 * pad_width
    group_width = pool_full.shape[0]
    position = offset + lax.iota(jnp.int32, n_tokens)
    column_pos = offset - pad_width + lax.iota(jnp.int32, padded.shape[0])
    center = padded[pad_width : pad_width + n_tokens].astype(jnp.float32)
    outputs = []
    for group_number, window_span in enumerate(pool_spans):
        low_edge = jnp.clip(position - window_span // 2, 0, seq_len)
        high_edge = jnp.clip(position - window_span // 2 + window_span, 0, seq_len)
        band_mask = (
            (column_pos[None, :] >= low_edge[:, None]) & (column_pos[None, :] < high_edge[:, None])
        ).astype(jnp.bfloat16)
        lower_col = group_number * group_width
        columns = padded[:, lower_col : lower_col + group_width]
        window_sum = jnp.dot(band_mask, columns, preferred_element_type=jnp.float32)
        window_mean = window_sum / (high_edge - low_edge).astype(jnp.float32)[:, None]
        deviation = (window_mean - center[:, lower_col : lower_col + group_width]).astype(
            jnp.bfloat16
        )
        mapped = jnp.dot(
            deviation, pool_full[:, group_number, :], preferred_element_type=jnp.float32
        )
        outputs.append(mapped + pool_bias[group_number])
    return jnp.concatenate(outputs, axis=-1) * pool_scale


def shards(
    tokens,
    gate_weight,
    up_weight,
    down_weight,
    pool_weight,
    pool_bias,
    pool_scale,
    gain_first,
    gain_mix,
    gain_second,
):
    gate_full, up_full, pool_half = (
        lax.all_gather(gate_weight, "fs", axis=0, tiled=True),
        lax.all_gather(up_weight, "fs", axis=0, tiled=True),
        lax.all_gather(pool_weight, "fs", axis=0, tiled=True),
    )
    down_full = lax.all_gather(down_weight, "fs", axis=1, tiled=True)
    pool_full = lax.all_gather(pool_half, "tp", axis=2, tiled=True)
    seq_len = tokens.shape[0]
    first_normed = rms_scale(tokens, gain_first)
    first_hidden = ffn_hidden(first_normed, gate_full, up_full)
    second_gate, second_up, second_down = (gate_full, up_full, down_full)
    first_branch = lax.psum(
        jnp.dot(first_hidden, down_full, preferred_element_type=jnp.float32).astype(jnp.bfloat16),
        "tp",
    ).astype(jnp.float32)
    after_first = (tokens.astype(jnp.float32) + 0.5 * first_branch).astype(jnp.bfloat16)
    mix_normed = rms_scale(after_first, gain_mix)
    padded = jnp.pad(mix_normed, ((pad_width, pad_width), (0, 0)))
    mixed = pool_block(padded, 0, seq_len, pool_full, pool_bias, pool_scale)
    after_mix = (after_first.astype(jnp.float32) + mixed).astype(jnp.bfloat16)
    second_normed = rms_scale(after_mix, gain_second)
    second_hidden = ffn_hidden(second_normed, second_gate, second_up)
    second_branch = lax.psum(
        jnp.dot(second_hidden, second_down, preferred_element_type=jnp.float32).astype(
            jnp.bfloat16
        ),
        "tp",
    ).astype(jnp.float32)
    return (after_mix.astype(jnp.float32) + 0.5 * second_branch).astype(jnp.bfloat16)


def solution(mesh):
    return jax.shard_map(
        shards,
        mesh=mesh,
        in_specs=(
            P(("grp", "fs"), None),
            P("fs", "tp"),
            P("fs", "tp"),
            P("tp", "fs"),
            P("fs", None, "tp"),
            P(),
            P(),
            P(),
            P(),
            P(),
        ),
        out_specs=P(("grp", "fs"), None),
        check_vma=False,
    )
```

profile of v0, /device:TPU:0, one launch (start us, length us, event | category | flops | bytes accessed | tf_op | source)
XLA Modules:
  0.0 468.3 jit_solution(4957366809883981244)
XLA Ops:
  6.5 0.0 copy-start
  6.5 0.0 copy-start.8
  6.5 0.0 all-gather.5.cloned.1.call-start
  6.5 0.7 all-gather.5.cloned.1.call-update
  7.3 0.0 all-gather.7.cloned.1.call-start
  7.3 0.7 all-gather.7.cloned.1.call-update
  8.0 0.0 all-gather.9.cloned.1.call-start
  8.1 0.7 all-gather.9.cloned.1.call-update
  8.7 0.0 all-reduce.4.cloned.1.call-start
  8.8 0.0 copy-done
  8.8 0.4 fusion
  9.2 100.5 %all-gather.5.cloned.1.call-done = bf16[2048,1280]{1,0:T(8,128)(2,1)} async-done(((bf16[512,1280]{1,0:T(8,128)(2,1)}), bf16[2048,1280]{1,0:T(8,128)(2,1)}) %all-gather.5.cloned.1.call-update) | async-done | bytes 5242896 | tf_op jit(solution)/shard_map/all_gather | solution.py:63
  109.7 0.0 copy-done.8
  109.7 6.0 %fusion.56 = f32[384,1280]{1,0:T(8,128)} fusion(bf16[2048,1280]{1,0:T(8,128)(2,1)} %all-gather.5.cloned.1.call-done, bf16[384,2048]{1,0:T(8,128)(2,1)S(1)} %copy-done, f32[2048]{0:T(1024)S(1)} %copy-done.8, f32[384]{0:T(512)S(1)} %add_rsqrt_fusion.2), kind=kOutput, calls=%fused_computation.69 | convolution fusion | flops 2016411648 | bytes 8791552 | tf_op jit(solution)/shard_map/dot_general | solution.py:18
  115.7 0.0 copy-start.4
  115.7 0.0 copy-start.7
  115.7 92.0 %all-gather.7.cloned.1.call-done = bf16[2048,1280]{1,0:T(8,128)(2,1)} async-done(((bf16[512,1280]{1,0:T(8,128)(2,1)}), bf16[2048,1280]{1,0:T(8,128)(2,1)}) %all-gather.7.cloned.1.call-update) | async-done | bytes 5242896 | tf_op jit(solution)/shard_map/all_gather | solution.py:64
  207.7 98.0 %all-gather.9.cloned.1.call-done = bf16[1280,2048]{1,0:T(8,128)(2,1)} async-done(((bf16[1280,512]{1,0:T(8,128)(2,1)}), bf16[1280,2048]{1,0:T(8,128)(2,1)}) %all-gather.9.cloned.1.call-update) | async-done | bytes 5242896 | tf_op jit(solution)/shard_map/all_gather | solution.py:67
  305.6 10.6 %convolution_convert_fusion.1 = bf16[384,2048]{1,0:T(8,128)(2,1)} fusion(bf16[1280,2048]{1,0:T(8,128)(2,1)} %all-gather.9.cloned.1.call-done, bf16[2048,1280]{1,0:T(8,128)(2,1)} %all-gather.7.cloned.1.call-done, f32[384,1280]{1,0:T(8,128)} %fusion.56, bf16[384,2048]{1,0:T(8,128)(2,1)S(1)} %copy-done, f32[2048]{0:T(1024)S(1)} %copy-done.8, ...), kind=kOutput, calls=%fused_computation.25 | convolution fusion | flops 4033413120 | bytes 15607296 | tf_op jit(solution)/shard_map/dot_general | solution.py:74
  316.3 0.0 copy-start.5
  316.3 0.0 all-reduce.4.cloned.1.call-update
  316.3 0.0 all-gather.11.cloned.1.call-start
  316.4 0.0 copy-done.4
  316.4 16.7 %all_gather.18 = bf16[512,4,128]{2,0,1:T(8,128)(2,1)} all-gather(bf16[128,4,128]{2,0,1:T(8,128)(2,1)S(1)} %copy.11), channel_id=1, replica_groups=mesh['grp'=2,'fs'=4,'tp'=4] {'fs'}, dimensions={0}, use_global_device_ids=true | all-gather | bytes 655360 | tf_op jit(solution)/shard_map/all_gather | solution.py:65
  333.1 0.0 all-gather.11.cloned.1.call-update
  333.1 0.2 all-reduce.6.cloned.1.call-start
  333.4 0.0 copy-done.7
  333.4 24.2 %all-reduce.4.cloned.1.call-done = bf16[384,2048]{1,0:T(8,128)(2,1)} async-done(((bf16[384,2048]{1,0:T(8,128)(2,1)}), bf16[384,2048]{1,0:T(8,128)(2,1)}) %all-reduce.4.cloned.1.call-update) | async-done | bytes 1572880 | tf_op jit(solution)/shard_map/psum | solution.py:73
  357.7 2.2 fusion.4
  359.9 0.0 copy-done.5
  359.9 0.0 copy-done.1
  359.9 3.0 fusion.97
  362.9 19.0 %all-gather.11.cloned.1.call-done = bf16[512,4,512]{2,0,1:T(8,128)(2,1)} async-done(((bf16[512,4,128]{2,0,1:T(8,128)(2,1)}), bf16[512,4,512]{2,0,1:T(8,128)(2,1)}) %all-gather.11.cloned.1.call-update) | async-done | bytes 2097168 | tf_op jit(solution)/shard_map/all_gather | solution.py:68
  382.0 3.0 convolution_add_fusion
  384.9 3.0 convolution_add_fusion.1
  387.9 3.0 convolution_add_fusion.2
  390.9 3.0 convolution_add_fusion.3
  393.9 0.0 copy-done.6
  393.9 2.9 fusion.8
  396.8 0.0 copy-start.2
  396.8 1.1 copy-done.2
  398.0 0.0 copy-done.9
  398.0 6.0 %fusion.52 = f32[384,1280]{1,0:T(8,128)} fusion(bf16[2048,1280]{1,0:T(8,128)(2,1)} %all-gather.5.cloned.1.call-done, bf16[384,2048]{1,0:T(8,128)(2,1)S(1)} %get-tuple-element.6, f32[2048]{0:T(1024)S(1)} %copy-done.9, f32[384]{0:T(512)S(1)} %add_rsqrt_fusion), kind=kOutput, calls=%fused_computation.68 | convolution fusion | flops 2016411648 | bytes 8791552 | tf_op jit(solution)/shard_map/dot_general | solution.py:18
  404.0 11.2 %convolution_convert_fusion = bf16[384,2048]{1,0:T(8,128)(2,1)} fusion(bf16[1280,2048]{1,0:T(8,128)(2,1)} %all-gather.9.cloned.1.call-done, bf16[2048,1280]{1,0:T(8,128)(2,1)} %all-gather.7.cloned.1.call-done, f32[384,1280]{1,0:T(8,128)} %fusion.52, bf16[384,2048]{1,0:T(8,128)(2,1)} %copy-done.2, f32[2048]{0:T(1024)S(1)} %copy-done.9, f32[384]{0:T(512)S(1)} %add_rsqrt_fusion), kind=kOutput, calls=%fused_computation.24 | convolution fusion | flops 4033413120 | bytes 15607296 | tf_op jit(solution)/shard_map/dot_general | solution.py:85
  415.2 0.0 all-reduce.6.cloned.1.call-update
  415.2 43.0 %all-reduce.6.cloned.1.call-done = bf16[384,2048]{1,0:T(8,128)(2,1)} async-done(((bf16[384,2048]{1,0:T(8,128)(2,1)}), bf16[384,2048]{1,0:T(8,128)(2,1)}) %all-reduce.6.cloned.1.call-update) | async-done | bytes 1572880 | tf_op jit(solution)/shard_map/psum | solution.py:84
  458.2 0.0 copy-done.3
  458.2 3.2 fusion.11
  (18 shorter events, 0.1 us)
Async XLA Ops:
  6.5 2.3 copy-start
  6.5 103.2 %copy-start.8 = (f32[2048]{0:T(1024)S(1)}, f32[2048]{0:T(1024)}, u32[]{:S(2)}) copy-start(f32[2048]{0:T(1024)} %param.17) | copy-start | bytes 24580
  6.5 103.2 %all-gather.5.cloned.1.call-start = ((), (), s32[]{:S(2)}) async-start(), calls=%async_computation | async-start | bytes 6553600 | tf_op jit(solution)/shard_map/all_gather | solution.py:63
  7.3 200.4 %all-gather.7.cloned.1.call-start = ((), (), s32[]{:S(2)}) async-start(), calls=%async_computation.1 | async-start | bytes 6553600 | tf_op jit(solution)/shard_map/all_gather | solution.py:64
  8.0 297.6 %all-gather.9.cloned.1.call-start = ((), (), s32[]{:S(2)}) async-start(), calls=%async_computation.2 | async-start | bytes 6553600 | tf_op jit(solution)/shard_map/all_gather | solution.py:67
  8.7 348.9 %all-reduce.4.cloned.1.call-start = ((), (), s32[]{:S(2)}) async-start(), calls=%async_computation.3 | async-start | bytes 3145728 | tf_op jit(solution)/shard_map/psum | solution.py:73
  115.7 200.7 %copy-start.4 = (bf16[128,4,128]{2,1,0:T(4,128)(2,1)S(1)}, bf16[128,4,128]{2,1,0:T(4,128)(2,1)}, u32[]{:S(2)}) copy-start(bf16[128,4,128]{2,1,0:T(4,128)(2,1)} %param.14) | copy-start | bytes 393220
  115.7 217.7 %copy-start.7 = (f32[4,512]{1,0:T(4,128)S(1)}, f32[4,512]{1,0:T(4,128)}, u32[]{:S(2)}) copy-start(f32[4,512]{1,0:T(4,128)} %param.15) | copy-start | bytes 24580
  316.3 43.6 %copy-start.5 = (f32[2048]{0:T(1024)S(1)}, f32[2048]{0:T(1024)}, u32[]{:S(2)}) copy-start(f32[2048]{0:T(1024)} %param.18) | copy-start | bytes 24580
  316.3 65.6 %all-gather.11.cloned.1.call-start = ((), (), s32[]{:S(2)}) async-start(), calls=%async_computation.4 | async-start | bytes 2621440 | tf_op jit(solution)/shard_map/all_gather | solution.py:68
  333.1 125.1 %all-reduce.6.cloned.1.call-start = ((), (), s32[]{:S(2)}) async-start(), calls=%async_computation.5 | async-start | bytes 3145728 | tf_op jit(solution)/shard_map/psum | solution.py:84
  357.6 2.2 copy-start.1
  390.9 3.0 copy-start.6
  393.9 4.1 copy-start.9
  396.8 1.1 copy-start.2
  404.0 54.2 %copy-start.3 = (bf16[384,2048]{1,0:T(8,128)(2,1)S(1)}, bf16[384,2048]{1,0:T(8,128)(2,1)}, u32[]{:S(2)}) copy-start(bf16[384,2048]{1,0:T(8,128)(2,1)} %copy-done.2) | copy-start | bytes 4718596
Sparse Core Ops, SparseCore 0:
  8.9 100.7 all-gather.4
  111.3 96.3 all-gather.6
  209.2 96.3 all-gather.8
  316.4 41.1 all-reduce.3
  359.0 22.8 all-gather.10
  415.3 42.8 all-reduce.5
where the time goes:
time: 469 us; the launch traced here: 468 us
  waiting for transfers between devices  379 us (81%)
  matrix products  45.8 us (10%)
  blocking collectives  16.7 us (4%)
  between operations  13.6 us (3%)
  other arithmetic  11.8 us (3%)
    all_gather x1, waiting for transfers between devices, shards(): lax.all_gather(gate_weight, 'fs', axis=0, tiled=True)  101 us
    all_gather x1, waiting for transfers between devices, shards(): down_full = lax.all_gather(down_weight, 'fs', axis=1, tiled=True)  98 us
    all_gather x1, waiting for transfers between devices, shards(): lax.all_gather(up_weight, 'fs', axis=0, tiled=True)  92 us
    psum x1, waiting for transfers between devices, shards(): lax.psum(jnp.dot(second_hidden, second_down, preferred_element_type=jnp.f...  43 us
    psum x1, waiting for transfers between devices, shards(): lax.psum(jnp.dot(first_hidden, down_full, preferred_element_type=jnp.floa...  24.2 us
    all_gather x1, waiting for transfers between devices, shards(): pool_full = lax.all_gather(pool_half, 'tp', axis=2, tiled=True)  19 us
    all_gather x1, blocking collectives, shards(): lax.all_gather(pool_weight, 'fs', axis=0, tiled=True)  16.7 us
    dot_general x2, matrix products, ffn_hidden(): gate_proj = jnp.dot(normed, gate_full, preferred_element_type=jnp.float32)  12 us
  transfers between devices with their start and end apart: 6, of which 6 were waited for; matrix products, arithmetic and copies ran while one was open for 3% of the time, Pallas kernels for 0%

commit v1 on v0

--- a/solution.py
+++ b/solution.py
@@ -64,7 +64,9 @@
         lax.all_gather(up_weight, "fs", axis=0, tiled=True),
         lax.all_gather(pool_weight, "fs", axis=0, tiled=True),
     )
-    down_full = lax.all_gather(down_weight, "fs", axis=1, tiled=True)
+    down_full = jnp.concatenate(
+        lax.all_to_all(jnp.stack([down_weight] * lax.axis_size("fs")), "fs", 0, 0), axis=1
+    )
     pool_full = lax.all_gather(pool_half, "tp", axis=2, tiled=True)
     seq_len = tokens.shape[0]
     first_normed = rms_scale(tokens, gain_first)

time: 469 us -> 469 us (level)
  waiting for transfers between devices: 379 us -> 369 us
  starting transfers between devices: 0.38 us -> 6.78 us
    all_gather x1 -> x0, waiting for transfers between devices: 98 us -> none  [shards(): down_full = lax.all_gather(down_weight, 'fs', axis=1, tiled=True)]
    all_gather x1, waiting for transfers between devices: 101 us -> 187 us  [shards(): lax.all_gather(gate_weight, 'fs', axis=0, tiled=True)]
    all_to_all x0 -> x1, starting transfers between devices: none -> 6.48 us  [shards(): lax.all_to_all(jnp.stack([down_weight] * lax.axis_size('fs')), 'fs', 0, 0)]
  transfers between devices with their start and end apart: 6 -> 6, of which waited for: 6 -> 5; matrix products, arithmetic and copies ran while one was open for 3% -> 3% of each run, Pallas kernels for 0% -> 0%
where the time goes in v1:
time: 469 us; the launch traced here: 468 us
  waiting for transfers between devices  369 us (79%)
  matrix products  45.8 us (10%)
  blocking collectives  16.6 us (4%)
  between operations  13.3 us (3%)
  other arithmetic  11.8 us (3%)
  starting transfers between devices  6.78 us (1%)
    all_gather x1, waiting for transfers between devices, shards(): lax.all_gather(gate_weight, 'fs', axis=0, tiled=True)  187 us
    all_gather x1, waiting for transfers between devices, shards(): lax.all_gather(up_weight, 'fs', axis=0, tiled=True)  94.4 us
    psum x1, waiting for transfers between devices, shards(): lax.psum(jnp.dot(second_hidden, second_down, preferred_element_type=jnp.f...  43 us
    psum x1, waiting for transfers between devices, shards(): lax.psum(jnp.dot(first_hidden, down_full, preferred_element_type=jnp.floa...  24.2 us
    all_gather x1, waiting for transfers between devices, shards(): pool_full = lax.all_gather(pool_half, 'tp', axis=2, tiled=True)  19.1 us
    all_gather x1, blocking collectives, shards(): lax.all_gather(pool_weight, 'fs', axis=0, tiled=True)  16.6 us
    dot_general x2, matrix products, ffn_hidden(): gate_proj = jnp.dot(normed, gate_full, preferred_element_type=jnp.float32)  12 us
    dot_general x4, matrix products, pool_block(): jnp.dot(deviation, pool_full[:, group_number, :], preferred_element_type=...  11.9 us
  transfers between devices with their start and end apart: 6, of which 5 were waited for; matrix products, arithmetic and copies ran while one was open for 3% of the time, Pallas kernels for 0%

profile of v1, /device:TPU:0, one launch (start us, length us, event | category | flops | bytes accessed | tf_op | source)
XLA Modules:
  0.0 468.2 jit_solution(13263021402348207091)
XLA Ops:
  6.5 0.0 copy-start.4
  6.5 0.0 all-gather.4.cloned.1.call-start
  6.5 0.7 all-gather.4.cloned.1.call-update
  7.3 0.0 all-gather.6.cloned.1.call-start
  7.3 0.7 all-gather.6.cloned.1.call-update
  8.0 0.0 copy-done.4
  8.0 0.6 copy.11
  8.6 2.6 stack.2
  11.2 0.0 copy-start
  11.2 0.0 copy-start.9
  11.2 6.5 %all-to-all-start = ((bf16[4,1280,512]{1,2,0:T(8,128)(2,1)}), bf16[4,1280,512]{1,2,0:T(8,128)(2,1)}, u32[]{:S(2)}, u32[]{:S(2)}) async-start(bf16[4,1280,512]{1,2,0:T(8,128)(2,1)} %stack.2), calls=%async_computation | async-start | bytes 10485760 | tf_op jit(solution)/shard_map/all_to_all | solution.py:68
  17.7 0.0 all-reduce.4.cloned.1.call-start
  17.7 0.0 copy-done
  17.7 0.4 fusion
  18.1 187.2 %all-gather.4.cloned.1.call-done = bf16[2048,1280]{1,0:T(8,128)(2,1)} async-done(((bf16[512,1280]{1,0:T(8,128)(2,1)}), bf16[2048,1280]{1,0:T(8,128)(2,1)}) %all-gather.4.cloned.1.call-update) | async-done | bytes 5242896 | tf_op jit(solution)/shard_map/all_gather | solution.py:63
  205.4 0.0 copy-done.9
  205.4 6.0 %fusion.56 = f32[384,1280]{1,0:T(8,128)} fusion(bf16[2048,1280]{1,0:T(8,128)(2,1)} %all-gather.4.cloned.1.call-done, bf16[384,2048]{1,0:T(8,128)(2,1)S(1)} %copy-done, f32[2048]{0:T(1024)S(1)} %copy-done.9, f32[384]{0:T(512)S(1)} %add_rsqrt_fusion.2), kind=kOutput, calls=%fused_computation.69 | convolution fusion | flops 2016411648 | bytes 8791552 | tf_op jit(solution)/shard_map/dot_general | solution.py:18
  211.4 94.4 %all-gather.6.cloned.1.call-done = bf16[2048,1280]{1,0:T(8,128)(2,1)} async-done(((bf16[512,1280]{1,0:T(8,128)(2,1)}), bf16[2048,1280]{1,0:T(8,128)(2,1)}) %all-gather.6.cloned.1.call-update) | async-done | bytes 5242896 | tf_op jit(solution)/shard_map/all_gather | solution.py:64
  305.8 0.0 all-to-all-done
  305.8 10.7 %convolution_convert_fusion.1 = bf16[384,2048]{1,0:T(8,128)(2,1)} fusion(bf16[1280,2048]{0,1:T(8,128)(2,1)} %bitcast.1, bf16[2048,1280]{1,0:T(8,128)(2,1)} %all-gather.6.cloned.1.call-done, f32[384,1280]{1,0:T(8,128)} %fusion.56, bf16[384,2048]{1,0:T(8,128)(2,1)S(1)} %copy-done, f32[2048]{0:T(1024)S(1)} %copy-done.9, f32[384]{0:T(512)S(1)} %add_rsqrt_fusion.2), kind=kOutput, calls=%fused_computation.25 | convolution fusion | flops 4033413120 | bytes 15607296 | tf_op jit(solution)/shard_map/dot_general | solution.py:76
  316.5 0.0 all-reduce.4.cloned.1.call-update
  316.5 0.0 all-gather.8.cloned.1.call-start
  316.6 0.0 copy-done.5
  316.6 16.6 %all_gather.14 = bf16[512,4,128]{2,0,1:T(8,128)(2,1)} all-gather(bf16[128,4,128]{2,0,1:T(8,128)(2,1)S(1)} %copy.12), channel_id=1, replica_groups=mesh['grp'=2,'fs'=4,'tp'=4] {'fs'}, dimensions={0}, use_global_device_ids=true | all-gather | bytes 655360 | tf_op jit(solution)/shard_map/all_gather | solution.py:65
  333.2 0.0 all-gather.8.cloned.1.call-update
  333.3 0.2 all-reduce.6.cloned.1.call-start
  333.6 0.0 copy-done.8
  333.6 24.2 %all-reduce.4.cloned.1.call-done = bf16[384,2048]{1,0:T(8,128)(2,1)} async-done(((bf16[384,2048]{1,0:T(8,128)(2,1)}), bf16[384,2048]{1,0:T(8,128)(2,1)}) %all-reduce.4.cloned.1.call-update) | async-done | bytes 1572880 | tf_op jit(solution)/shard_map/psum | solution.py:75
  357.8 2.2 fusion.4
  360.1 0.0 copy-done.6
  360.1 0.0 copy-done.1
  360.1 3.0 fusion.97
  363.1 19.1 %all-gather.8.cloned.1.call-done = bf16[512,4,512]{2,0,1:T(8,128)(2,1)} async-done(((bf16[512,4,128]{2,0,1:T(8,128)(2,1)}), bf16[512,4,512]{2,0,1:T(8,128)(2,1)}) %all-gather.8.cloned.1.call-update) | async-done | bytes 2097168 | tf_op jit(solution)/shard_map/all_gather | solution.py:70
  382.2 3.0 convolution_add_fusion
  385.1 3.0 convolution_add_fusion.1
  388.1 3.0 convolution_add_fusion.2
  391.1 3.0 convolution_add_fusion.3
  394.1 0.0 copy-done.7
  394.1 2.9 fusion.8
  397.0 0.0 copy-start.2
  397.0 1.1 copy-done.2
  398.2 0.0 copy-done.10
  398.2 6.0 %fusion.52 = f32[384,1280]{1,0:T(8,128)} fusion(bf16[2048,1280]{1,0:T(8,128)(2,1)} %all-gather.4.cloned.1.call-done, bf16[384,2048]{1,0:T(8,128)(2,1)S(1)} %get-tuple-element.6, f32[2048]{0:T(1024)S(1)} %copy-done.10, f32[384]{0:T(512)S(1)} %add_rsqrt_fusion), kind=kOutput, calls=%fused_computation.68 | convolution fusion | flops 2016411648 | bytes 8791552 | tf_op jit(solution)/shard_map/dot_general | solution.py:18
  404.2 11.2 %convolution_convert_fusion = bf16[384,2048]{1,0:T(8,128)(2,1)} fusion(bf16[1280,2048]{0,1:T(8,128)(2,1)} %bitcast.1, bf16[2048,1280]{1,0:T(8,128)(2,1)} %all-gather.6.cloned.1.call-done, f32[384,1280]{1,0:T(8,128)} %fusion.52, bf16[384,2048]{1,0:T(8,128)(2,1)} %copy-done.2, f32[2048]{0:T(1024)S(1)} %copy-done.10, f32[384]{0:T(512)S(1)} %add_rsqrt_fusion), kind=kOutput, calls=%fused_computation.24 | convolution fusion | flops 4033413120 | bytes 15607296 | tf_op jit(solution)/shard_map/dot_general | solution.py:87
  415.4 0.0 all-reduce.6.cloned.1.call-update
  415.4 43.0 %all-reduce.6.cloned.1.call-done = bf16[384,2048]{1,0:T(8,128)(2,1)} async-done(((bf16[384,2048]{1,0:T(8,128)(2,1)}), bf16[384,2048]{1,0:T(8,128)(2,1)}) %all-reduce.6.cloned.1.call-update) | async-done | bytes 1572880 | tf_op jit(solution)/shard_map/psum | solution.py:86
  458.4 0.0 copy-done.3
  458.4 3.2 fusion.11
  (21 shorter events, 0.1 us)
Async XLA Ops:
  6.5 1.5 copy-start.4
  6.5 198.8 %all-gather.4.cloned.1.call-start = ((), (), s32[]{:S(2)}) async-start(), calls=%async_computation.1 | async-start | bytes 6553600 | tf_op jit(solution)/shard_map/all_gather | solution.py:63
  7.3 298.5 %all-gather.6.cloned.1.call-start = ((), (), s32[]{:S(2)}) async-start(), calls=%async_computation.2 | async-start | bytes 6553600 | tf_op jit(solution)/shard_map/all_gather | solution.py:64
  11.2 6.5 %copy-start = (bf16[384,2048]{1,0:T(8,128)(2,1)S(1)}, bf16[384,2048]{1,0:T(8,128)(2,1)}, u32[]{:S(2)}) copy-start(bf16[384,2048]{1,0:T(8,128)(2,1)} %param.10) | copy-start | bytes 4718596
  11.2 194.1 %copy-start.9 = (f32[2048]{0:T(1024)S(1)}, f32[2048]{0:T(1024)}, u32[]{:S(2)}) copy-start(f32[2048]{0:T(1024)} %param.17) | copy-start | bytes 24580
  11.2 294.6 %all-to-all-start = ((bf16[4,1280,512]{1,2,0:T(8,128)(2,1)}), bf16[4,1280,512]{1,2,0:T(8,128)(2,1)}, u32[]{:S(2)}, u32[]{:S(2)}) async-start(bf16[4,1280,512]{1,2,0:T(8,128)(2,1)} %stack.2), calls=%async_computation | async-start | bytes 10485760 | tf_op jit(solution)/shard_map/all_to_all | solution.py:68
  17.7 340.1 %all-reduce.4.cloned.1.call-start = ((), (), s32[]{:S(2)}) async-start(), calls=%async_computation.3 | async-start | bytes 3145728 | tf_op jit(solution)/shard_map/psum | solution.py:75
  305.8 10.8 %copy-start.5 = (bf16[128,4,128]{2,1,0:T(4,128)(2,1)S(1)}, bf16[128,4,128]{2,1,0:T(4,128)(2,1)}, u32[]{:S(2)}) copy-start(bf16[128,4,128]{2,1,0:T(4,128)(2,1)} %param.14) | copy-start | bytes 393220
  305.8 27.8 %copy-start.8 = (f32[4,512]{1,0:T(4,128)S(1)}, f32[4,512]{1,0:T(4,128)}, u32[]{:S(2)}) copy-start(f32[4,512]{1,0:T(4,128)} %param.15) | copy-start | bytes 24580
  316.5 43.6 %copy-start.6 = (f32[2048]{0:T(1024)S(1)}, f32[2048]{0:T(1024)}, u32[]{:S(2)}) copy-start(f32[2048]{0:T(1024)} %param.18) | copy-start | bytes 24580
  316.5 65.7 %all-gather.8.cloned.1.call-start = ((), (), s32[]{:S(2)}) async-start(), calls=%async_computation.4 | async-start | bytes 2621440 | tf_op jit(solution)/shard_map/all_gather | solution.py:70
  333.3 125.1 %all-reduce.6.cloned.1.call-start = ((), (), s32[]{:S(2)}) async-start(), calls=%async_computation.5 | async-start | bytes 3145728 | tf_op jit(solution)/shard_map/psum | solution.py:86
  357.8 2.2 copy-start.1
  391.1 3.0 copy-start.7
  394.1 4.1 copy-start.10
  397.0 1.1 copy-start.2
  404.2 54.2 %copy-start.3 = (bf16[384,2048]{1,0:T(8,128)(2,1)S(1)}, bf16[384,2048]{1,0:T(8,128)(2,1)}, u32[]{:S(2)}) copy-start(bf16[384,2048]{1,0:T(8,128)(2,1)} %copy-done.2) | copy-start | bytes 4718596
Sparse Core Ops, SparseCore 0:
  8.9 196.4 all-gather.3
  206.9 98.8 all-gather.5
  316.6 41.1 all-reduce.3
  359.3 22.8 all-gather.7
  415.5 42.8 all-reduce.5
